TPU v7x, 256 devices: a whole 4x4x8 slice. The times are simulated.
256 devices in a mesh: sp: 16 (over y, x), tp: 16 (over z, core).
Axes of the slice: x: 4, y: 4, z: 8, core: 2. Of those that a mesh axis runs over, the one named last changes fastest.
Arguments:
- queries: bfloat16 [8192, 2048], P('sp', 'tp'), may hold values from -16 to 16
- key_vectors: bfloat16 [8192, 2048], P('sp', 'tp'), may hold values from -4 to 4
- value_vectors: bfloat16 [8192, 2048], P('sp', 'tp'), may hold values from -5 to 5
- forget_totals: float32 [8192, 16], P('sp', 'tp'), may hold values from -1368 to 0, as said below
- head_gain: float32 [2048], P('tp'), may hold values from 0.1 to 1.9
- stream: bfloat16 [8192, 2048], P(('sp', 'tp')), may hold values from -6 to 6
- out_weight: bfloat16 [2048, 2048], replicated, may hold values from -0.125 to 0.125
- norm_gain: float32 [2048], replicated, may hold values from 0.1 to 1.9
- routing: int32 [8192, 2], P(('sp', 'tp')), may hold values from 0 to 15, all different within a row; in each aligned block of 32 rows (0 to 31, 32 to 63, ...) at most 8 rows name the same one
- route_weights: float32 [8192, 2], P(('sp', 'tp')), may hold values from 0.2 to 1
- gate_weight: bfloat16 [16, 2048, 4096], P('sp', None, 'tp'), may hold values from -0.125 to 0.125
- up_weight: bfloat16 [16, 2048, 4096], P('sp', None, 'tp'), may hold values from -0.125 to 0.125
- down_weight: bfloat16 [16, 4096, 2048], P('sp', 'tp'), may hold values from -0.09375 to 0.09375
Outputs:
- layer_out: bfloat16 [8192, 2048], P(('sp', 'tp'))
Inputs may be any that keep to these rules, and one draw needn't show every extreme that they name: `forget_totals`: along the positions, the values of each head never rise. `routing`: A token's 2 experts differ. Within the tokens of one device (aligned blocks of 32 rows) no expert is named more than 8 times.
All inputs are finite; a program needn't handle non-finite values.
Results may differ from a plain program's by a relative error of at most 0.01145.
Values may be sent and summed in bfloat16 or wider, within the bound.
A program may use at most 128 MiB of HBM per device.

v0:
```python
from functools import partial

import jax
import jax.numpy as jnp
from jax import lax
from jax.sharding import PartitionSpec as P

HD = 128
TOP = 2


masked_score = -1e30


def sent_together(arrays, axis, dim, along):
    ends, at = ([], 0)
    for a in arrays[:-1]:
        at += a.shape[along]
        ends.append(at)
    both = jnp.concatenate(arrays, axis=along)
    return tuple(jnp.split(lax.all_gather(both, axis, axis=dim, tiled=True), ends, axis=along))


def attend_block(
    totals, query_rows, query_gate, query_pos, key_rows, value_rows, key_gate, key_pos
):
    run_max, run_sum, run_acc = totals
    scores = jnp.einsum("qhd,khd->hqk", query_rows, key_rows, preferred_element_type=jnp.float32)
    scores = scores * HD ** (-0.5) + query_gate[:, :, None] - key_gate[:, None, :]
    visible = (key_pos[None, :] <= query_pos[:, None])[None]
    scores = jnp.where(visible, scores, masked_score)
    new_max = jnp.maximum(run_max, jnp.max(scores, axis=2))
    lifted = jnp.where(visible, jnp.exp(scores - new_max[:, :, None]), 0.0)
    rescale = jnp.exp(run_max - new_max)
    new_sum = run_sum * rescale + jnp.sum(lifted, axis=2)
    product = jnp.einsum(
        "hqk,khd->hqd", lifted.astype(jnp.bfloat16), value_rows, preferred_element_type=jnp.float32
    )
    new_acc = run_acc * rescale[:, :, None] + product
    return (new_max, new_sum, new_acc)


def keep_totals(totals_in):
    return totals_in


def make_folder(segments, gathered_gates):

    def fold_keys(state_all, key_piece, first_key):
        key_part, value_part = key_piece
        key_total = key_part.shape[0]
        block_len = min(512, key_total)
        heads_dev = segments[0][0].shape[1]
        key_part = key_part.reshape(key_total, heads_dev, HD)
        value_part = value_part.reshape(key_total, heads_dev, HD)

        def one_block(block_index, state_now):
            offset = block_index * block_len
            key_rows = lax.dynamic_slice_in_dim(key_part, offset, block_len, 0)
            value_rows = lax.dynamic_slice_in_dim(value_part, offset, block_len, 0)
            key_pos = offset + jnp.arange(block_len, dtype=jnp.int32)
            key_gate = jnp.transpose(lax.dynamic_slice_in_dim(gathered_gates, offset, block_len, 0))
            updated = []
            for segment, totals_in in zip(segments, state_now):
                query_rows, query_gate, query_pos = segment
                needed = offset <= query_pos[-1]
                advance = partial(
                    attend_block,
                    query_rows=query_rows,
                    query_gate=query_gate,
                    query_pos=query_pos,
                    key_rows=key_rows,
                    value_rows=value_rows,
                    key_gate=key_gate,
                    key_pos=key_pos,
                )
                updated.append(lax.cond(needed, advance, keep_totals, totals_in))
            return tuple(updated)

        return lax.fori_loop(0, key_total // block_len, one_block, state_all)

    return fold_keys


def on_device(
    queries,
    key_vectors,
    value_vectors,
    forget_totals,
    head_gain,
    stream,
    out_weight,
    norm_gain,
    routing,
    route_weights,
    gate_weight,
    up_weight,
    down_weight,
):
    tok_count = queries.shape[0]
    heads_dev = queries.shape[1] // HD
    sp_index = lax.axis_index("sp")
    sp_count = lax.axis_size("sp")
    gathered_gates = lax.all_gather(forget_totals, "sp", axis=0, tiled=True)
    first_pos = sp_index * tok_count
    query_pos = first_pos + jnp.arange(tok_count, dtype=jnp.int32)
    query_gate = jnp.transpose(lax.dynamic_slice_in_dim(gathered_gates, first_pos, tok_count, 0))
    segments = [(queries.reshape(tok_count, heads_dev, HD), query_gate, query_pos)]
    starting = (
        (
            jnp.full((heads_dev, tok_count), masked_score, jnp.float32),
            jnp.zeros((heads_dev, tok_count), jnp.float32),
            jnp.zeros((heads_dev, tok_count, HD), jnp.float32),
        ),
    )
    folder = make_folder(segments, gathered_gates)
    totals = folder(starting, sent_together((key_vectors, value_vectors), "sp", 0, 1), jnp.int32(0))
    run_max, run_sum, run_acc = totals[0]
    attended = run_acc / run_sum[:, :, None]
    inverse_rms = lax.rsqrt(jnp.mean(attended * attended, axis=2, keepdims=True) + 1e-06)
    normed = attended * inverse_rms * head_gain.reshape(heads_dev, 1, HD)
    head_out = (
        jnp.transpose(normed, (1, 0, 2)).reshape(tok_count, heads_dev * HD).astype(jnp.bfloat16)
    )
    token_heads = lax.all_to_all(head_out, "tp", split_axis=0, concat_axis=1, tiled=True)
    mixed_rows = jnp.dot(token_heads, out_weight, preferred_element_type=jnp.float32)
    resid_sum = stream.astype(jnp.float32) + mixed_rows
    center = resid_sum - jnp.mean(resid_sum, axis=1, keepdims=True)
    normed_rows = (
        center * lax.rsqrt(jnp.mean(center * center, axis=1, keepdims=True) + 1e-05) * norm_gain
    ).astype(jnp.bfloat16)
    row_count = normed_rows.shape[0]
    capacity = max(2, 2 * TOP * row_count // sp_count)
    flat_expert = routing.reshape(-1)
    onehot = (flat_expert[:, None] == jnp.arange(sp_count, dtype=jnp.int32)[None, :]).astype(
        jnp.int32
    )
    earlier = jnp.cumsum(onehot, axis=0) - onehot
    slot_index = flat_expert * capacity + jnp.sum(earlier * onehot, axis=1)
    slot_grid = slot_index.reshape(row_count, TOP)
    slot_ids = jnp.arange(sp_count * capacity, dtype=jnp.int32)
    placing = jnp.sum(
        (slot_grid[None, :, :] == slot_ids[:, None, None]).astype(jnp.float32), axis=2
    ).astype(jnp.bfloat16)
    outgoing = jnp.dot(placing, normed_rows, preferred_element_type=jnp.float32).astype(
        jnp.bfloat16
    )
    outgoing = outgoing.reshape(sp_count, capacity, normed_rows.shape[1])
    arrived = lax.all_to_all(outgoing, "sp", split_axis=0, concat_axis=0, tiled=True)
    row_piece = lax.all_gather(arrived.reshape(-1, arrived.shape[2]), "tp", axis=0, tiled=True)
    gate_pre = jnp.dot(row_piece, gate_weight[0], preferred_element_type=jnp.float32)
    up_pre = jnp.dot(row_piece, up_weight[0], preferred_element_type=jnp.float32)
    hidden = (jax.nn.silu(gate_pre) * up_pre).astype(jnp.bfloat16)
    summed = lax.psum_scatter(
        jnp.dot(hidden, down_weight[0], preferred_element_type=jnp.float32).astype(jnp.bfloat16),
        "tp",
        scatter_dimension=0,
        tiled=True,
    )
    expert_out = summed.reshape(sp_count, capacity, -1)
    returned = lax.all_to_all(expert_out, "sp", split_axis=0, concat_axis=0, tiled=True)
    picked = returned.reshape(sp_count * capacity, -1)[slot_index].astype(jnp.float32)
    weighted = picked * route_weights.reshape(-1)[:, None]
    routed = jnp.sum(weighted.reshape(row_count, TOP, -1), axis=1)
    return (resid_sum + routed).astype(jnp.bfloat16)


def solution(mesh):
    in_specs = (
        P("sp", "tp"),
        P("sp", "tp"),
        P("sp", "tp"),
        P("sp", "tp"),
        P("tp"),
        P(("sp", "tp"), None),
        P(),
        P(),
        P(("sp", "tp"), None),
        P(("sp", "tp"), None),
        P("sp", None, "tp"),
        P("sp", None, "tp"),
        P("sp", "tp", None),
    )
    out_specs = P(("sp", "tp"), None)
    return jax.shard_map(
        on_device, mesh=mesh, in_specs=in_specs, out_specs=out_specs, check_vma=False
    )
```

profile of v0, /device:TPU:2, one launch (start us, length us, event | category | flops | bytes accessed | tf_op | source)
XLA Modules:
  0.0 334.1 jit_solution(2829663943095619503)
XLA Ops:
  6.5 1.8 pad_maximum_fusion
  8.3 0.8 copy.26
  9.7 23.4 %all_gather.10 = f32[8192,1]{0,1:T(1,128)S(1)} all-gather(f32[512,1]{0,1:T(1,128)} %param.20), channel_id=1, replica_groups=mesh['sp'=16,'tp'=16] {'sp'}, dimensions={0}, use_global_device_ids=true | all-gather | bytes 34816 | tf_op jit(solution)/shard_map/all_gather | solution.py:104
  33.1 36.1 %all-gather.3.cloned.1.call-done = bf16[8192,256]{1,0:T(8,128)(2,1)} async-done(((bf16[512,256]{1,0:T(8,128)(2,1)}), bf16[8192,256]{1,0:T(8,128)(2,1)}) %all-gather.3.cloned.1.call-update) | async-done | bytes 4194320 | tf_op jit(solution)/shard_map/all_gather | solution.py:21
  69.2 3.8 %slice_bitcast_fusion = (bf16[8192,1,128]{2,0,1:T(8,128)(2,1)S(1)}, bf16[8192,1,128]{2,0,1:T(8,128)(2,1)}) fusion(bf16[8192,256]{1,0:T(8,128)(2,1)} %all-gather.3.cloned.1.call-done), kind=kLoop, calls=%fused_computation.33 | loop fusion | bytes 8388608 | tf_op jit(solution)/shard_map/reshape | solution.py:55
  73.1 23.5 %while.17 = (s32[]{:T(128)}, f32[1,512]{1,0:T(1,128)S(1)}, f32[1,512]{1,0:T(1,128)S(1)}, f32[1,512,128]{2,1,0:T(8,128)S(1)}, s32[512]{0:T(512)S(1)}, /*index=5*/...) while((s32[]{:T(128)}, f32[1,512]{1,0:T(1,128)S(1)}, ...), condition=%wide.region_5.6_spmd, body=%wide.region_0.5_spmd.sunk | while | flops 138020352 | bytes 4122969 | solution.py:80
  74.3 2.2 conditional.2
  74.3 1.4 fusion.38
  77.7 2.2 conditional.2
  77.7 1.4 fusion.38
  96.8 0.9 multiply_convert_fusion.1
  97.7 7.1 %all-to-all-start = ((bf16[16,32,128]{2,1,0:T(8,128)(2,1)}), bf16[16,32,128]{2,1,0:T(8,128)(2,1)S(1)}, u32[]{:S(2)}, u32[]{:S(2)}) async-start(bf16[16,32,128]{2,1,0:T(8,128)(2,1)} %bitcast.16), calls=%async_computation | async-start | bytes 262144 | tf_op jit(solution)/shard_map/all_to_all | solution.py:125
  105.1 8.4 %all-to-all-done = bf16[16,32,128]{2,1,0:T(8,128)(2,1)S(1)} async-done(((bf16[16,32,128]{2,1,0:T(8,128)(2,1)}), bf16[16,32,128]{2,1,0:T(8,128)(2,1)S(1)}, u32[]{:S(2)}, u32[]{:S(2)}) %all-to-all-start) | async-done | bytes 131104 | tf_op jit(solution)/shard_map/all_to_all | solution.py:125
  113.5 5.0 %fusion.39 = (f32[32]{0:T(128)S(1)}, f32[32,2048]{1,0:T(8,128)S(1)}) fusion(bf16[2048,2048]{1,0:T(8,128)(2,1)} %param.23, bf16[32,2048]{1,0:T(8,128)(2,1)} %param.22, bf16[16,32,128]{2,1,0:T(8,128)(2,1)S(1)} %all-to-all-done), kind=kOutput, calls=%fused_computation.72 | convolution fusion | flops 268632032 | bytes 8913024 | tf_op jit(solution)/shard_map/dot_general | solution.py:126
  119.1 46.6 %all_to_all.26 = bf16[16,8,2048]{2,1,0:T(8,128)(2,1)} all-to-all(bf16[16,8,2048]{2,1,0:T(8,128)(2,1)S(1)} %fusion.21), channel_id=1, replica_groups=mesh['sp'=16,'tp'=16] {'sp'}, dimensions={0} | all-to-all | bytes 1048576 | tf_op jit(solution)/shard_map/all_to_all | solution.py:149
  165.8 49.9 %all-gather.5.cloned.1.call-done = bf16[2048,2048]{1,0:T(8,128)(2,1)} async-done(((bf16[128,2048]{1,0:T(8,128)(2,1)}), bf16[2048,2048]{1,0:T(8,128)(2,1)}) %all-gather.5.cloned.1.call-update) | async-done | bytes 8388624 | tf_op jit(solution)/shard_map/all_gather | solution.py:150
  215.8 7.1 %fusion.25 = f32[2048,256]{1,0:T(8,128)} fusion(bf16[2048,2048]{1,0:T(8,128)(2,1)} %all-gather.5.cloned.1.call-done, bf16[1,2048,256]{2,1,0:T(8,128)(2,1)S(1)} %copy-done.4), kind=kOutput, calls=%fused_computation.37 | convolution fusion | flops 2147483648 | bytes 11534336 | tf_op jit(solution)/shard_map/dot_general | solution.py:151
  222.9 16.8 %convolution_convert_fusion = bf16[2048,2048]{1,0:T(8,128)(2,1)} fusion(bf16[2048,2048]{1,0:T(8,128)(2,1)} %all-gather.5.cloned.1.call-done, f32[2048,256]{1,0:T(8,128)} %fusion.25, bf16[1,256,2048]{2,1,0:T(8,128)(2,1)S(1)} %copy-done, bf16[1,2048,256]{2,1,0:T(8,128)(2,1)} %param.28), kind=kOutput, calls=%fused_computation.27 | convolution fusion | flops 4302307328 | bytes 20971520 | tf_op jit(solution)/shard_map/dot_general | solution.py:155
  239.7 69.3 %reduce-scatter.2.cloned.1.call-done = bf16[128,2048]{1,0:T(8,128)(2,1)} async-done(((bf16[2048,2048]{1,0:T(8,128)(2,1)}), bf16[128,2048]{1,0:T(8,128)(2,1)}) %reduce-scatter.2.cloned.1.call-update) | async-done | bytes 524304 | tf_op jit(solution)/shard_map/reduce_scatter | solution.py:154
  309.0 7.3 %all-to-all-start.2 = ((bf16[16,8,2048]{2,1,0:T(8,128)(2,1)}), bf16[16,8,2048]{2,1,0:T(8,128)(2,1)S(1)}, u32[]{:S(2)}, u32[]{:S(2)}) async-start(bf16[16,8,2048]{2,1,0:T(8,128)(2,1)} %bitcast.76), calls=%async_computation.3 | async-start | bytes 1048576 | tf_op jit(solution)/shard_map/all_to_all | solution.py:161
  316.5 8.6 %all-to-all-done.2 = bf16[16,8,2048]{2,1,0:T(8,128)(2,1)S(1)} async-done(((bf16[16,8,2048]{2,1,0:T(8,128)(2,1)}), bf16[16,8,2048]{2,1,0:T(8,128)(2,1)S(1)}, u32[]{:S(2)}, u32[]{:S(2)}) %all-to-all-start.2) | async-done | bytes 524320 | tf_op jit(solution)/shard_map/all_to_all | solution.py:161
  325.1 0.7 gather_fusion
  326.2 0.7 multiply_reduce_fusion
  326.9 0.7 add_convert_fusion
  (100 shorter events, 13.3 us)
Async XLA Ops:
  6.5 216.3 %copy-start = (bf16[1,256,2048]{2,1,0:T(8,128)(2,1)S(1)}, bf16[1,256,2048]{2,1,0:T(8,128)(2,1)}, u32[]{:S(2)}) copy-start(bf16[1,256,2048]{2,1,0:T(8,128)(2,1)} %param.29) | copy-start | bytes 3145732
  6.5 62.7 %all-gather.3.cloned.1.call-start = ((), (), s32[]{:S(2)}) async-start(), calls=%async_computation.4 | async-start | bytes 4456448 | tf_op jit(solution)/shard_map/all_gather | solution.py:21
  73.1 23.8 %copy-start.3 = (f32[128]{0:T(128)S(1)}, f32[128]{0:T(128)}, u32[]{:S(2)}) copy-start(f32[128]{0:T(128)} %param.21) | copy-start | bytes 1540
  97.7 15.8 %all-to-all-start = ((bf16[16,32,128]{2,1,0:T(8,128)(2,1)}), bf16[16,32,128]{2,1,0:T(8,128)(2,1)S(1)}, u32[]{:S(2)}, u32[]{:S(2)}) async-start(bf16[16,32,128]{2,1,0:T(8,128)(2,1)} %bitcast.16), calls=%async_computation | async-start | bytes 262144 | tf_op jit(solution)/shard_map/all_to_all | solution.py:125
  104.8 110.9 %all-gather.5.cloned.1.call-start = ((), (), s32[]{:S(2)}) async-start(), calls=%async_computation.5 | async-start | bytes 8912896 | tf_op jit(solution)/shard_map/all_gather | solution.py:150
  105.1 13.7 %copy-start.1 = (f32[2048]{0:T(1024)S(1)}, f32[2048]{0:T(1024)}, u32[]{:S(2)}) copy-start(f32[2048]{0:T(1024)} %param.24) | copy-start | bytes 24580
  118.5 97.3 %copy-start.4 = (bf16[1,2048,256]{2,1,0:T(8,128)(2,1)S(1)}, bf16[1,2048,256]{2,1,0:T(8,128)(2,1)}, u32[]{:S(2)}) copy-start(bf16[1,2048,256]{2,1,0:T(8,128)(2,1)} %param.27) | copy-start | bytes 3145732
  165.8 143.2 %reduce-scatter.2.cloned.1.call-start = ((), (), s32[]{:S(2)}) async-start(), calls=%async_computation.6 | async-start | bytes 8912896 | tf_op jit(solution)/shard_map/reduce_scatter | solution.py:154
  239.7 76.8 %copy-start.2 = (f32[32,2]{0,1:T(2,128)S(1)}, f32[32,2]{0,1:T(2,128)}, u32[]{:S(2)}) copy-start(f32[32,2]{0,1:T(2,128)} %param.26) | copy-start | bytes 772
  309.0 16.1 %all-to-all-start.2 = ((bf16[16,8,2048]{2,1,0:T(8,128)(2,1)}), bf16[16,8,2048]{2,1,0:T(8,128)(2,1)S(1)}, u32[]{:S(2)}, u32[]{:S(2)}) async-start(bf16[16,8,2048]{2,1,0:T(8,128)(2,1)} %bitcast.76), calls=%async_computation.3 | async-start | bytes 1048576 | tf_op jit(solution)/shard_map/all_to_all | solution.py:161
Sparse Core Ops, SparseCore 0:
  9.8 59.4 all-gather.2
  165.9 49.8 all-gather.4
  239.8 69.1 reduce-scatter.1
where the time goes:
time: 335 us; the launch traced here: 334 us
  waiting for transfers between devices  172 us (51%)
  blocking collectives  70.1 us (21%)
  matrix products  33 us (10%)
  local copies, waits for them, and re-layouts  15.5 us (5%)
  starting transfers between devices  14.5 us (4%)
  between operations  13.3 us (4%)
  loops' own time  9.92 us (3%)
  other arithmetic  5.49 us (2%)
    reduce_scatter x1, waiting for transfers between devices, on_device(): lax.psum_scatter(jnp.dot(hidden, down_weight[0], preferred_element_type=j...  69.3 us
    all_gather x1, waiting for transfers between devices, on_device(): lax.all_gather(arrived.reshape(-1, arrived.shape[2]), 'tp', axis=0, tiled...  49.9 us
    all_to_all x1, blocking collectives, on_device(): lax.all_to_all(outgoing, 'sp', split_axis=0, concat_axis=0, tiled=True)  46.6 us
    all_gather x1, waiting for transfers between devices, sent_together(): lax.all_gather(both, axis, axis=dim, tiled=True)  36.1 us
    all_gather x1, blocking collectives, on_device(): gathered_gates = lax.all_gather(forget_totals, 'sp', axis=0, tiled=True)  23.4 us
    dot_general x1, matrix products, on_device(): jnp.dot(hidden, down_weight[0], preferred_element_type=jnp.float32)  16.8 us
    another operation x1, loops' own time, fold_keys(): return lax.fori_loop(0, key_total // block_len, one_block, state_all)  9.6 us
    slice x16, local copies, waits for them, and re-layouts, one_block(): needed = offset <= query_pos[-1]  9.2 us
  transfers between devices with their start and end apart: 5, of which 5 were waited for; matrix products, arithmetic and copies ran while one was open for 1% of the time, Pallas kernels for 0%

commit v1 on v0

v1 whole, which is shorter than its diff:
```python
from functools import partial

import jax
import jax.numpy as jnp
from jax import lax
from jax.experimental import pallas as pl
from jax.experimental.pallas import tpu as pltpu
from jax.sharding import PartitionSpec as P

HD = 128
TOP = 2
SIDE = 4
MESH = pl.DeviceIdType.MESH
F32 = jnp.float32
BF16 = jnp.bfloat16
LOG2E = 1.4426950408889634
HIDDEN_SCORE = -1e30


def attention_kernel(
    tp_count,
    q_ref,
    k_ref,
    v_ref,
    g_ref,
    head_gain_ref,
    stream_ref,
    norm_gain_ref,
    out_w_ref,
    resid_ref,
    normed_ref,
    kb,
    vb,
    gb,
    m_ref,
    acc_ref,
    ho,
    th,
    w_buf,
    kv_send,
    kv_recv,
    g_send,
    g_recv,
    h_send,
    h_recv,
    w_sem,
):
    tok = q_ref.shape[0]
    half = tok // 2
    rows = stream_ref.shape[0]
    sp_count = SIDE * SIDE
    me = lax.axis_index("sp")
    tpi = lax.axis_index("tp")
    mx = me % SIDE
    my = me // SIDE

    def sp_of(x, y):
        return (y % SIDE) * SIDE + x % SIDE

    fetch_w = pltpu.make_async_copy(out_w_ref, w_buf, w_sem)
    fetch_w.start()

    barrier = pltpu.get_barrier_semaphore()

    @pl.loop(1, sp_count)
    def _(j):
        pl.semaphore_signal(
            barrier, inc=1, device_id=((me + j) % sp_count, tpi), device_id_type=MESH
        )

    @pl.loop(1, tp_count)
    def _(j):
        pl.semaphore_signal(
            barrier, inc=1, device_id=(me, (tpi + j) % tp_count), device_id_type=MESH
        )

    pl.semaphore_wait(barrier, sp_count - 1 + tp_count - 1)

    def piece(ref, blk, part):
        if part is None:
            return ref.at[blk]
        return ref.at[blk, pl.ds(part * half, half), :]

    def place(kind, a, b):
        return sp_of(a, b) if kind == 0 else sp_of(b, a)

    def copy(kind, idx, block, part, target):
        buf = (kb, vb)[kind]
        own = (k_ref, v_ref)[kind]
        ma, mb = (mx, my) if kind == 0 else (my, mx)
        blk = place(kind, ma + block[0], mb + block[1])
        if block == (0, 0):
            src = own if part is None else own.at[pl.ds(part * half, half), :]
        else:
            src = piece(buf, blk, part)
        return pltpu.make_async_remote_copy(
            src_ref=src,
            dst_ref=piece(buf, blk, part),
            send_sem=kv_send.at[kind, idx],
            recv_sem=kv_recv.at[kind, idx],
            device_id=(place(kind, ma + target[0], mb + target[1]), tpi),
            device_id_type=MESH,
        )

    plan = {
        0: ((0, 0), None, (1, 0)),
        1: ((0, 0), None, (-1, 0)),
        2: ((-1, 0), 0, (1, 0)),
        3: ((1, 0), 1, (-1, 0)),
    }
    for n, a in enumerate((0, -1, 1, 2)):
        plan[4 + 4 * n] = ((a, 0), None, (0, 1))
        plan[5 + 4 * n] = ((a, 0), None, (0, -1))
        plan[6 + 4 * n] = ((a, -1), 0, (0, 1))
        plan[7 + 4 * n] = ((a, 1), 1, (0, -1))

    def send(kind, idx):
        block, part, target = plan[idx]
        copy(kind, idx, block, part, target).start()

    def arrive(kind, idx):
        block, part, target = plan[idx]
        buf = (kb, vb)[kind]
        ma, mb = (mx, my) if kind == 0 else (my, mx)
        blk = place(kind, ma + block[0] - target[0], mb + block[1] - target[1])
        pltpu.make_async_remote_copy(
            src_ref=piece(buf, blk, part),
            dst_ref=piece(buf, blk, part),
            send_sem=kv_send.at[kind, idx],
            recv_sem=kv_recv.at[kind, idx],
            device_id=(place(kind, ma + target[0], mb + target[1]), tpi),
            device_id_type=MESH,
        ).wait_recv()

    def gate_copy(j, blk_out):
        return pltpu.make_async_remote_copy(
            src_ref=g_ref,
            dst_ref=gb.at[blk_out],
            send_sem=g_send.at[j - 1],
            recv_sem=g_recv.at[j - 1],
            device_id=((me + j) % sp_count, tpi),
            device_id_type=MESH,
        )

    for idx in (0, 1):
        send(0, idx)
    for idx in (0, 1):
        send(1, idx)

    @pl.loop(1, sp_count)
    def _(j):
        gate_copy(j, me).start()

    for idx in (4, 5):
        send(0, idx)
    for idx in (4, 5):
        send(1, idx)

    scale = HD ** (-0.5) * LOG2E
    part_rows = min(256, tok)
    reps = tok // HD

    def fold(k_blk, v_blk, g_row, first):
        v_ones = jnp.concatenate([v_blk, jnp.ones((tok, HD), BF16)], axis=1)
        for r in range(tok // part_rows):
            rs = pl.ds(r * part_rows, part_rows)
            s = lax.dot_general(
                q_ref[rs, :], k_blk, (((1,), (1,)), ((), ())), preferred_element_type=F32
            )
            t = s * scale + g_row
            if first:
                keys = lax.broadcasted_iota(jnp.int32, (part_rows, tok), 1)
                qs = lax.broadcasted_iota(jnp.int32, (part_rows, tok), 0) + r * part_rows
                t = jnp.where(keys <= qs, t, HIDDEN_SCORE)
            top = jnp.max(t, axis=1, keepdims=True)
            if first:
                m_new = jnp.broadcast_to(top, (part_rows, HD))
            else:
                m_old = m_ref[rs, :]
                m_new = jnp.maximum(m_old, top)
            p = jnp.exp2(t - jnp.concatenate([m_new] * reps, axis=1))
            pv = jnp.dot(p.astype(BF16), v_ones, preferred_element_type=F32)
            if first:
                acc_ref[rs, :] = pv
            else:
                alpha = jnp.exp2(m_old - m_new)
                acc_ref[rs, :] = acc_ref[rs, :] * jnp.concatenate([alpha] * 2, axis=1) + pv
            m_ref[rs, :] = m_new

    fold(k_ref[...], v_ref[...], g_ref[...], True)

    @pl.loop(1, sp_count)
    def _(i):
        @pl.when(i == 1)
        def _():
            for kind in (0, 1):
                arrive(kind, 0)
                for idx in (2, 8, 9):
                    send(kind, idx)
                arrive(kind, 1)
                for idx in (3, 12, 13):
                    send(kind, idx)
            for kind in (0, 1):
                arrive(kind, 4)
                send(kind, 6)
                arrive(kind, 5)
                send(kind, 7)

            @pl.loop(1, sp_count)
            def _(j):
                gate_copy(j, (me + sp_count - j) % sp_count).wait_recv()

        @pl.when(i == 5)
        def _():
            for kind in (0, 1):
                arrive(kind, 2)
                arrive(kind, 3)
                for idx in (16, 17):
                    send(kind, idx)
            for kind in (0, 1):
                for got, idx in ((8, 10), (9, 11), (12, 14), (13, 15)):
                    arrive(kind, got)
                    send(kind, idx)
            for kind in (0, 1):
                arrive(kind, 6)
                arrive(kind, 7)

        @pl.when(i == 11)
        def _():
            for kind in (0, 1):
                for got, idx in ((16, 18), (17, 19)):
                    arrive(kind, got)
                    send(kind, idx)
            for kind in (0, 1):
                for got in (10, 11, 14, 15):
                    arrive(kind, got)

        @pl.when(i == 15)
        def _():
            for kind in (0, 1):
                arrive(kind, 18)
                arrive(kind, 19)

        def since(n):
            return (i + 16 - n) // 16

        j1, j2, j3, j4 = i - 1 + 16, i - 5, i - 7 + 16, i - 11 + 16
        w1 = since(1) - since(5)
        w2 = since(5) - since(7)
        w3 = since(7) - since(11)
        w4 = since(11) - since(15)
        w5 = since(15)
        h1, p1 = (j1 - 16 + 16) // 2 - 8, 1 + 2 * (j1 % 2)
        p3, q3 = 1 + 2 * (j3 % 2), 1 + 2 * (j3 // 2 - 8)
        h4, p4 = j4 // 2 - 8, 1 + 2 * (j4 % 2)
        dx = (
            w1 * (1 - h1) * p1
            + w2 * 2 * (1 - j2)
            + w3 * p3
            + w4 * ((1 - h4) * 2 + h4 * p4)
            + w5 * 2
        )
        dy = w1 * h1 * p1 + w2 * 2 * j2 + w3 * q3 + w4 * ((1 - h4) * p4 + h4 * 2) + w5 * 2
        blk = sp_of(mx + dx, my + dy)

        @pl.when(blk < me)
        def _():
            fold(kb[blk], vb[blk], gb[blk], False)

    total = acc_ref[...]
    attended = total[:, :HD] / total[:, HD:]
    rms = lax.rsqrt(jnp.mean(attended * attended, axis=1, keepdims=True) + 1e-06)
    ho[...] = (attended * rms * head_gain_ref[...]).astype(BF16)

    def head_copy(j, block):
        to = (tpi + j) % tp_count
        return pltpu.make_async_remote_copy(
            src_ref=ho.at[pl.ds(pl.multiple_of(to * rows, rows), rows), :],
            dst_ref=th.at[block],
            send_sem=h_send.at[j - 1],
            recv_sem=h_recv.at[j - 1],
            device_id=(me, to),
            device_id_type=MESH,
        )

    @pl.loop(1, tp_count)
    def _(j):
        head_copy(j, tpi).start()

    for kind in (0, 1):
        for idx in range(20):
            block, part, target = plan[idx]
            copy(kind, idx, block, part, target).wait_send()

    @pl.loop(1, sp_count)
    def _(j):
        gate_copy(j, me).wait_send()

    th[tpi] = ho[pl.ds(pl.multiple_of(tpi * rows, rows), rows), :]
    fetch_w.wait()

    @pl.loop(1, tp_count)
    def _(j):
        head_copy(j, (tpi + tp_count - j) % tp_count).wait_recv()

    heads = jnp.concatenate([th[t] for t in range(tp_count)], axis=1)
    width = out_w_ref.shape[1]
    step = min(512, width)

    @pl.loop(0, width // step)
    def _(n):
        cols = pl.ds(pl.multiple_of(n * step, step), step)
        resid_ref[:, cols] = stream_ref[:, cols].astype(F32) + jnp.dot(
            heads, w_buf[:, cols], preferred_element_type=F32
        )

    resid = resid_ref[...]
    center = resid - jnp.mean(resid, axis=1, keepdims=True)
    spread = lax.rsqrt(jnp.mean(center * center, axis=1, keepdims=True) + 1e-05)
    normed_ref[...] = (center * spread * norm_gain_ref[...]).astype(BF16)

    @pl.loop(1, tp_count)
    def _(j):
        head_copy(j, tpi).wait_send()


def attention_part(
    tp_count, queries, key_vectors, value_vectors, forget_totals, head_gain, stream, out_weight, norm_gain
):
    tok = queries.shape[0]
    rows, width = stream.shape
    sp_count = SIDE * SIDE
    gates = (forget_totals * (-LOG2E)).reshape(1, tok)
    in_vmem = pl.BlockSpec(memory_space=pltpu.VMEM)
    return pl.pallas_call(
        partial(attention_kernel, tp_count),
        name="attention",
        out_shape=(
            jax.ShapeDtypeStruct((rows, width), F32),
            jax.ShapeDtypeStruct((rows, width), BF16),
        ),
        in_specs=[in_vmem] * 7 + [pl.BlockSpec(memory_space=pl.ANY)],
        out_specs=(in_vmem, in_vmem),
        scratch_shapes=[
            pltpu.VMEM((sp_count, tok, HD), BF16),
            pltpu.VMEM((sp_count, tok, HD), BF16),
            pltpu.VMEM((sp_count, 1, tok), F32),
            pltpu.VMEM((tok, HD), F32),
            pltpu.VMEM((tok, 2 * HD), F32),
            pltpu.VMEM((tok, HD), BF16),
            pltpu.VMEM((tp_count, rows, HD), BF16),
            pltpu.VMEM(out_weight.shape, BF16),
            pltpu.SemaphoreType.DMA((2, 20)),
            pltpu.SemaphoreType.DMA((2, 20)),
            pltpu.SemaphoreType.DMA((sp_count - 1,)),
            pltpu.SemaphoreType.DMA((sp_count - 1,)),
            pltpu.SemaphoreType.DMA((tp_count - 1,)),
            pltpu.SemaphoreType.DMA((tp_count - 1,)),
            pltpu.SemaphoreType.DMA,
        ],
        compiler_params=pltpu.CompilerParams(
            collective_id=0, has_side_effects=True, vmem_limit_bytes=48 * 1024 * 1024
        ),
    )(
        queries,
        key_vectors,
        value_vectors,
        gates,
        head_gain.reshape(1, HD),
        stream,
        norm_gain.reshape(1, width),
        out_weight,
    )


def on_device(
    tp_count,
    queries,
    key_vectors,
    value_vectors,
    forget_totals,
    head_gain,
    stream,
    out_weight,
    norm_gain,
    routing,
    route_weights,
    gate_weight,
    up_weight,
    down_weight,
):
    sp_count = lax.axis_size("sp")
    resid_sum, normed_rows = attention_part(
        tp_count,
        queries,
        key_vectors,
        value_vectors,
        forget_totals,
        head_gain,
        stream,
        out_weight,
        norm_gain,
    )
    row_count = normed_rows.shape[0]
    capacity = max(2, 2 * TOP * row_count // sp_count)
    flat_expert = routing.reshape(-1)
    onehot = (flat_expert[:, None] == jnp.arange(sp_count, dtype=jnp.int32)[None, :]).astype(
        jnp.int32
    )
    earlier = jnp.cumsum(onehot, axis=0) - onehot
    slot_index = flat_expert * capacity + jnp.sum(earlier * onehot, axis=1)
    slot_grid = slot_index.reshape(row_count, TOP)
    slot_ids = jnp.arange(sp_count * capacity, dtype=jnp.int32)
    placing = jnp.sum(
        (slot_grid[None, :, :] == slot_ids[:, None, None]).astype(jnp.float32), axis=2
    ).astype(jnp.bfloat16)
    outgoing = jnp.dot(placing, normed_rows, preferred_element_type=jnp.float32).astype(
        jnp.bfloat16
    )
    outgoing = outgoing.reshape(sp_count, capacity, normed_rows.shape[1])
    arrived = lax.all_to_all(outgoing, "sp", split_axis=0, concat_axis=0, tiled=True)
    row_piece = lax.all_gather(arrived.reshape(-1, arrived.shape[2]), "tp", axis=0, tiled=True)
    gate_pre = jnp.dot(row_piece, gate_weight[0], preferred_element_type=jnp.float32)
    up_pre = jnp.dot(row_piece, up_weight[0], preferred_element_type=jnp.float32)
    hidden = (jax.nn.silu(gate_pre) * up_pre).astype(jnp.bfloat16)
    summed = lax.psum_scatter(
        jnp.dot(hidden, down_weight[0], preferred_element_type=jnp.float32).astype(jnp.bfloat16),
        "tp",
        scatter_dimension=0,
        tiled=True,
    )
    expert_out = summed.reshape(sp_count, capacity, -1)
    returned = lax.all_to_all(expert_out, "sp", split_axis=0, concat_axis=0, tiled=True)
    picked = returned.reshape(sp_count * capacity, -1)[slot_index].astype(jnp.float32)
    weighted = picked * route_weights.reshape(-1)[:, None]
    routed = jnp.sum(weighted.reshape(row_count, TOP, -1), axis=1)
    return (resid_sum + routed).astype(jnp.bfloat16)


def solution(mesh):
    in_specs = (
        P("sp", "tp"),
        P("sp", "tp"),
        P("sp", "tp"),
        P("sp", "tp"),
        P("tp"),
        P(("sp", "tp"), None),
        P(),
        P(),
        P(("sp", "tp"), None),
        P(("sp", "tp"), None),
        P("sp", None, "tp"),
        P("sp", None, "tp"),
        P("sp", "tp", None),
    )
    out_specs = P(("sp", "tp"), None)
    return jax.shard_map(
        partial(on_device, mesh.shape["tp"]),
        mesh=mesh,
        in_specs=in_specs,
        out_specs=out_specs,
        check_vma=False,
    )
```

time: 335 us -> 242 us (0.72)
  blocking collectives: 70.1 us -> 17.2 us
  Pallas kernels: 0 us -> 43.3 us
  waiting for transfers between devices: 172 us -> 130 us
  matrix products: 33 us -> 20.5 us
  loops' own time: 9.92 us -> 0 us
  local copies, waits for them, and re-layouts: 15.5 us -> 7.3 us
  starting transfers between devices: 14.5 us -> 7.34 us
    pallas_call x0 -> x1, Pallas kernels: none -> 43.3 us  [attention_part(): pl.pallas_call(partial(attention_kernel, tp_count), name='attention', out...]
    all_gather x1 -> x0, waiting for transfers between devices: 36.1 us -> none  [sent_together(): lax.all_gather(both, axis, axis=dim, tiled=True)]
    all_to_all x1, blocking collectives: 46.6 us -> 17.2 us  [on_device(): lax.all_to_all(outgoing, 'sp', split_axis=0, concat_axis=0, tiled=True)]
    all_gather x1 -> x0, blocking collectives: 23.4 us -> none  [on_device(): gathered_gates = lax.all_gather(forget_totals, 'sp', axis=0, tiled=True)]
    another operation x17 -> x0, loops' own time: 9.92 us -> none  [the longest x1 9.6 us: fold_keys(): return lax.fori_loop(0, key_total // block_len, one_block, state_all)]
    slice x16 -> x0, local copies, waits for them, and re-layouts: 9.2 us -> none  [one_block(): needed = offset <= query_pos[-1]]
    dot_general x5 -> x0, matrix products: 8.79 us -> none  [the longest x1 5.03 us: on_device(): jnp.dot(token_heads, out_weight, preferred_element_type=jnp.float32)]
    all_to_all x1 -> x0, waiting for transfers between devices: 8.41 us -> none  [on_device(): lax.all_to_all(head_out, 'tp', split_axis=0, concat_axis=1, tiled=True)]
  transfers between devices with their start and end apart: 5 -> 3, of which waited for: 5 -> 3; matrix products, arithmetic and copies ran while one was open for 1% -> 0% of each run, Pallas kernels for 0% -> 0%
where the time goes in v1:
time: 242 us; the launch traced here: 241 us
  waiting for transfers between devices  130 us (54%)
  Pallas kernels  43.3 us (18%)
  matrix products  20.5 us (8%)
  blocking collectives  17.2 us (7%)
  between operations  13.5 us (6%)
  starting transfers between devices  7.34 us (3%)
  local copies, waits for them, and re-layouts  7.3 us (3%)
  other arithmetic  2.64 us (1%)
    reduce_scatter x1, waiting for transfers between devices, on_device(): lax.psum_scatter(jnp.dot(hidden, down_weight[0], preferred_element_type=j...  69.3 us
    all_gather x1, waiting for transfers between devices, on_device(): lax.all_gather(arrived.reshape(-1, arrived.shape[2]), 'tp', axis=0, tiled...  51.7 us
    pallas_call x1, Pallas kernels, attention_part(): pl.pallas_call(partial(attention_kernel, tp_count), name='attention', out...  43.3 us
    all_to_all x1, blocking collectives, on_device(): lax.all_to_all(outgoing, 'sp', split_axis=0, concat_axis=0, tiled=True)  17.2 us
    dot_general x1, matrix products, on_device(): jnp.dot(hidden, down_weight[0], preferred_element_type=jnp.float32)  13.1 us
    all_to_all x1, waiting for transfers between devices, on_device(): lax.all_to_all(expert_out, 'sp', split_axis=0, concat_axis=0, tiled=True)  8.56 us
    all_to_all x1, starting transfers between devices, on_device(): lax.all_to_all(expert_out, 'sp', split_axis=0, concat_axis=0, tiled=True)  7.3 us
    dot_general x1, matrix products, on_device(): jnp.dot(row_piece, gate_weight[0], preferred_element_type=jnp.float32)  7.08 us
  transfers between devices with their start and end apart: 3, of which 3 were waited for; matrix products, arithmetic and copies ran while one was open for 0% of the time, Pallas kernels for 0%

profile of v1, /device:TPU:2, one launch (start us, length us, event | category | flops | bytes accessed | tf_op | source)
XLA Modules:
  0.0 241.4 jit_solution(17129387320674616342)
XLA Ops:
  6.5 0.8 multiply_bitcast_fusion.g_ref
  7.3 0.8 copy.20
  8.1 0.1 eq.28
  8.4 0.2 select_reduce_fusion
  8.5 0.1 reduce_sum.32
  8.8 0.9 copy-done.1
  9.7 0.9 copy-done.2
  10.6 0.9 copy-done.3
  11.5 0.9 copy-done.4
  12.5 0.7 copy-done.5
  13.1 0.7 copy-done.6
  13.8 43.3 %attention.1 = (f32[32,2048]{1,0:T(8,128)S(1)}, bf16[32,2048]{1,0:T(8,128)(2,1)S(1)}) custom-call(bf16[512,128]{1,0:T(8,128)(2,1)S(1)} %copy-done.1, bf16[512,128]{1,0:T(8,128)(2,1)S(1)} %copy-done.2, bf16[512,128]{1,0:T(8,128)(2,1)S(1)} %copy-done.3, f32[1,512]{1,0:T(1,128)S(1)} %multiply_bitcast_fusion.g_ref, f32[1,128]{1,0:T(1,128)S(1)} %bitcast.30, ...), custom_call_target="tpu_custom_call" | custom-call | tf_op jit(solution)/shard_map/attention/pallas_call | solution.py:335
  57.1 0.3 fusion.1
  57.4 17.2 %all_to_all.10 = bf16[16,8,2048]{2,1,0:T(8,128)(2,1)} all-to-all(bf16[16,8,2048]{2,1,0:T(8,128)(2,1)S(1)} %fusion.1), channel_id=1, replica_groups=mesh['sp'=16,'tp'=16] {'sp'}, dimensions={0} | all-to-all | bytes 1048576 | tf_op jit(solution)/shard_map/all_to_all | solution.py:421
  74.7 51.7 %all-gather.2.cloned.1.call-done = bf16[2048,2048]{1,0:T(8,128)(2,1)} async-done(((bf16[128,2048]{1,0:T(8,128)(2,1)}), bf16[2048,2048]{1,0:T(8,128)(2,1)}) %all-gather.2.cloned.1.call-update) | async-done | bytes 8388624 | tf_op jit(solution)/shard_map/all_gather | solution.py:422
  126.4 7.1 %fusion.5 = f32[2048,256]{1,0:T(8,128)} fusion(bf16[2048,2048]{1,0:T(8,128)(2,1)} %all-gather.2.cloned.1.call-done, bf16[1,2048,256]{2,1,0:T(8,128)(2,1)S(1)} %copy-done.8), kind=kOutput, calls=%fused_computation.8 | convolution fusion | flops 2147483648 | bytes 11534336 | tf_op jit(solution)/shard_map/dot_general | solution.py:423
  133.4 13.1 %convolution_convert_fusion = bf16[2048,2048]{1,0:T(8,128)(2,1)} fusion(bf16[2048,2048]{1,0:T(8,128)(2,1)} %all-gather.2.cloned.1.call-done, f32[2048,256]{1,0:T(8,128)} %fusion.5, bf16[1,256,2048]{2,1,0:T(8,128)(2,1)S(1)} %copy-done, bf16[1,2048,256]{2,1,0:T(8,128)(2,1)S(1)} %copy-done.9), kind=kOutput, calls=%fused_computation.1 | convolution fusion | flops 4302307328 | bytes 20971520 | tf_op jit(solution)/shard_map/dot_general | solution.py:427
  146.6 69.3 %reduce-scatter.2.cloned.1.call-done = bf16[128,2048]{1,0:T(8,128)(2,1)} async-done(((bf16[2048,2048]{1,0:T(8,128)(2,1)}), bf16[128,2048]{1,0:T(8,128)(2,1)}) %reduce-scatter.2.cloned.1.call-update) | async-done | bytes 524304 | tf_op jit(solution)/shard_map/reduce_scatter | solution.py:426
  215.9 7.3 %all-to-all-start.1 = ((bf16[16,8,2048]{2,1,0:T(8,128)(2,1)}), bf16[16,8,2048]{2,1,0:T(8,128)(2,1)S(1)}, u32[]{:S(2)}, u32[]{:S(2)}) async-start(bf16[16,8,2048]{2,1,0:T(8,128)(2,1)} %bitcast.33), calls=%async_computation.2 | async-start | bytes 1048576 | tf_op jit(solution)/shard_map/all_to_all | solution.py:433
  223.5 8.6 %all-to-all-done.1 = bf16[16,8,2048]{2,1,0:T(8,128)(2,1)S(1)} async-done(((bf16[16,8,2048]{2,1,0:T(8,128)(2,1)}), bf16[16,8,2048]{2,1,0:T(8,128)(2,1)S(1)}, u32[]{:S(2)}, u32[]{:S(2)}) %all-to-all-start.1) | async-done | bytes 524320 | tf_op jit(solution)/shard_map/all_to_all | solution.py:433
  232.0 0.7 gather_fusion
  232.8 0.3 reshape.74
  233.1 0.7 multiply_reduce_fusion
  233.8 0.7 add_convert_fusion
  (27 shorter events, 0.6 us)
Async XLA Ops:
  6.5 126.9 %copy-start = (bf16[1,256,2048]{2,1,0:T(8,128)(2,1)S(1)}, bf16[1,256,2048]{2,1,0:T(8,128)(2,1)}, u32[]{:S(2)}) copy-start(bf16[1,256,2048]{2,1,0:T(8,128)(2,1)} %param.25) | copy-start | bytes 3145732
  6.5 119.8 %all-gather.2.cloned.1.call-start = ((), (), s32[]{:S(2)}) async-start(), calls=%async_computation.3 | async-start | bytes 8912896 | tf_op jit(solution)/shard_map/all_gather | solution.py:422
  8.8 0.9 copy-start.1
  9.7 0.9 copy-start.2
  10.6 0.9 copy-start.3
  11.5 0.9 copy-start.4
  12.4 0.7 copy-start.5
  13.1 0.7 copy-start.6
  13.8 112.6 %copy-start.8 = (bf16[1,2048,256]{2,1,0:T(8,128)(2,1)S(1)}, bf16[1,2048,256]{2,1,0:T(8,128)(2,1)}, u32[]{:S(2)}) copy-start(bf16[1,2048,256]{2,1,0:T(8,128)(2,1)} %param.23) | copy-start | bytes 3145732
  74.6 58.8 %copy-start.9 = (bf16[1,2048,256]{2,1,0:T(8,128)(2,1)S(1)}, bf16[1,2048,256]{2,1,0:T(8,128)(2,1)}, u32[]{:S(2)}) copy-start(bf16[1,2048,256]{2,1,0:T(8,128)(2,1)} %param.24) | copy-start | bytes 3145732
  74.6 141.3 %reduce-scatter.2.cloned.1.call-start = ((), (), s32[]{:S(2)}) async-start(), calls=%async_computation.4 | async-start | bytes 8912896 | tf_op jit(solution)/shard_map/reduce_scatter | solution.py:426
  146.6 76.8 %copy-start.7 = (f32[32,2]{0,1:T(2,128)S(1)}, f32[32,2]{0,1:T(2,128)}, u32[]{:S(2)}) copy-start(f32[32,2]{0,1:T(2,128)} %param.22) | copy-start | bytes 772
  215.9 16.1 %all-to-all-start.1 = ((bf16[16,8,2048]{2,1,0:T(8,128)(2,1)}), bf16[16,8,2048]{2,1,0:T(8,128)(2,1)S(1)}, u32[]{:S(2)}, u32[]{:S(2)}) async-start(bf16[16,8,2048]{2,1,0:T(8,128)(2,1)} %bitcast.33), calls=%async_computation.2 | async-start | bytes 1048576 | tf_op jit(solution)/shard_map/all_to_all | solution.py:433
Sparse Core Ops, SparseCore 0:
  74.7 51.5 all-gather.1
  146.7 69.1 reduce-scatter.1
